TPU v7x, 32 devices: a whole 2x2x4 slice. The times are simulated.
32 devices in a mesh: sp: 8 (over z, x), tp: 4 (over y, core).
Axes of the slice: x: 2, y: 2, z: 4, core: 2. Of those that a mesh axis runs over, the one named last changes fastest.
Arguments:
- tokens: bfloat16 [6144, 2048], P(('sp', 'tp')), may hold values from -6 to 6
- in_gain: float32 [2048], replicated, may hold values from 0.1 to 1.9
- w_query: bfloat16 [2048, 1024], P(None, 'tp'), may hold values from -0.125 to 0.125
- w_key: bfloat16 [2048, 1024], P(None, 'tp'), may hold values from -0.125 to 0.125
- w_value: bfloat16 [2048, 2048], P(None, 'tp'), may hold values from -0.125 to 0.125
- w_input_gate: bfloat16 [2048, 8], replicated, may hold values from -8 to 8
- w_forget_gate: bfloat16 [2048, 8], replicated, may hold values from -0.125 to 0.125
- forget_bias: float32 [8], replicated
- forget_extra: float32 [6144, 8], P('sp', 'tp'), may hold values from -2 to 0
- w_conv_gate: bfloat16 [2048, 2048], P(None, 'tp'), may hold values from -0.125 to 0.125
- w_conv_left: bfloat16 [2048, 2048], P(None, 'tp'), may hold values from -0.125 to 0.125
- w_conv_right: bfloat16 [2048, 2048], P(None, 'tp'), may hold values from -0.125 to 0.125
- conv_taps: float32 [3, 2048], replicated, may hold values from -3.5 to 3.5
- first_memory: float32 [8, 128, 256], P('tp'), may hold values from -2560 to 2560
- first_norm: float32 [8, 128], P('tp'), may hold values from -2560 to 2560
- w_out_memory: bfloat16 [2048, 2048], P('tp'), may hold values from -0.09375 to 0.09375
- w_out_conv: bfloat16 [2048, 2048], P('tp'), may hold values from -0.09375 to 0.09375
Outputs:
- mixed: bfloat16 [6144, 2048], P(('sp', 'tp'))
All inputs are finite; a program needn't handle non-finite values.
Results may differ from a plain program's by a relative error of at most 0.015.
The roundings to bfloat16 on the way count: a program that leaves them out, or rounds other values in their place, can miss the bound.
Values may be sent and summed in bfloat16 or wider, within the bound.
A program may use at most 64 MiB of HBM per device.

v0:
```python
import jax
import jax.numpy as jnp
from jax import lax
from jax.sharding import PartitionSpec as P

KEY_DIM = 128
VALUE_DIM = 256
TAPS = 3
V_WIDTH = 2048


epsilon = 1e-06
very_negative = -1e30
highest = lax.Precision.HIGHEST


def from_behind(block, axis, distance):
    devices = range(lax.axis_size(axis))
    route = [(i - distance, i) for i in devices if i - distance in devices]
    return lax.ppermute(block, axis, route)


def entering(part, axis, combine, identity):
    place = lax.axis_index(axis)
    gathered = jax.tree.map(lambda a: lax.all_gather(a, axis), part)
    state = jax.tree.map(lambda a, e: jnp.zeros_like(a) + jnp.asarray(e, a.dtype), part, identity)

    def one(turn, state):
        return combine(
            state, jax.tree.map(lambda a: lax.dynamic_index_in_dim(a, turn, 0, False), gathered)
        )

    return lax.fori_loop(0, place, one, state)


def rounded(values):
    return lax.optimization_barrier(values.astype(jnp.bfloat16)).astype(jnp.float32)


def join_states(earlier, later):
    decay_early, max_early, memory_early, norm_early = earlier
    decay_late, max_late, memory_late, norm_late = later
    joined_max = jnp.maximum(max_early + decay_late, max_late)
    scale_early = jnp.exp(max_early + decay_late - joined_max)
    scale_late = jnp.exp(max_late - joined_max)
    joined_memory = (
        scale_early[:, None, None] * memory_early + scale_late[:, None, None] * memory_late
    )
    joined_norm = scale_early[:, None] * norm_early + scale_late[:, None] * norm_late
    return (decay_early + decay_late, joined_max, joined_memory, joined_norm)


def per_device(
    tokens,
    in_gain,
    w_query,
    w_key,
    w_value,
    w_input_gate,
    w_forget_gate,
    forget_bias,
    forget_extra,
    w_conv_gate,
    w_conv_left,
    w_conv_right,
    conv_taps,
    first_memory,
    first_norm,
    w_out_memory,
    w_out_conv,
):
    heads_here = w_query.shape[1] // KEY_DIM
    query_width = heads_here * KEY_DIM
    value_width = heads_here * VALUE_DIM
    channels = w_conv_gate.shape[1]
    head_first = lax.axis_index("tp") * heads_here
    channel_first = lax.axis_index("tp") * channels
    input_gate = lax.dynamic_slice_in_dim(w_input_gate, head_first, heads_here, 1)
    forget_gate = lax.dynamic_slice_in_dim(w_forget_gate, head_first, heads_here, 1)
    bias_here = lax.dynamic_slice_in_dim(forget_bias, head_first, heads_here, 0)
    taps_here = lax.dynamic_slice_in_dim(conv_taps, channel_first, channels, 1)
    token_rows = tokens.astype(jnp.float32)
    scale_rows = lax.rsqrt(jnp.mean(token_rows * token_rows, axis=1, keepdims=True) + epsilon)
    normed = (token_rows * scale_rows * in_gain).astype(jnp.bfloat16)
    sub_rows = lax.all_gather(normed, "tp", axis=0, tiled=True)
    pieces = [
        jnp.dot(sub_rows, weight, preferred_element_type=jnp.float32)
        for weight in (
            w_query,
            w_key,
            w_value,
            w_conv_gate,
            w_conv_left,
            w_conv_right,
            input_gate,
            forget_gate,
        )
    ]
    projected = jnp.concatenate(pieces, axis=1)
    row_count = projected.shape[0]
    offset_value = 2 * query_width
    offset_conv = offset_value + value_width
    offset_gate = offset_conv + 3 * channels
    query_rows = (
        projected[:, 0:query_width].astype(jnp.bfloat16).reshape(row_count, heads_here, KEY_DIM)
    )
    key_rows = (
        projected[:, query_width:offset_value]
        .astype(jnp.bfloat16)
        .reshape(row_count, heads_here, KEY_DIM)
    )
    value_rows = (
        projected[:, offset_value:offset_conv]
        .astype(jnp.bfloat16)
        .reshape(row_count, heads_here, VALUE_DIM)
    )
    conv_gate = rounded(projected[:, offset_conv : offset_conv + channels])
    conv_left = rounded(projected[:, offset_conv + channels : offset_conv + 2 * channels])
    conv_right = rounded(projected[:, offset_conv + 2 * channels : offset_gate])
    in_pre = projected[:, offset_gate : offset_gate + heads_here]
    forget_pre = projected[:, offset_gate + heads_here : offset_gate + 2 * heads_here] + bias_here
    log_forget = jax.nn.log_sigmoid(forget_pre) + forget_extra
    cumulative = jnp.cumsum(log_forget, axis=0)
    decay_total = cumulative[row_count - 1]
    weight_log = decay_total[None, :] - cumulative + in_pre
    block_max = jnp.max(weight_log, axis=0)
    keyed = key_rows.astype(jnp.float32) * jnp.exp(weight_log - block_max[None, :])[:, :, None]
    block_norm = jnp.sum(keyed, axis=0)
    block_memory = jnp.einsum(
        "shd,shv->hdv", keyed.astype(jnp.bfloat16), value_rows, preferred_element_type=jnp.float32
    )
    product = (conv_left * conv_right).astype(jnp.bfloat16)
    edge_rows = product[row_count - (TAPS - 1) :]
    before_rows = from_behind(edge_rows, "sp", 1)
    prior_decay, prior_max, prior_memory, prior_norm = entering(
        (decay_total, block_max, block_memory, block_norm),
        "sp",
        join_states,
        (
            jnp.zeros_like(decay_total),
            jnp.full_like(block_max, very_negative),
            jnp.zeros_like(block_memory),
            jnp.zeros_like(block_norm),
        ),
    )
    enter_max = jnp.maximum(prior_max, prior_decay)
    from_prior = jnp.exp(prior_max - enter_max)
    from_first = jnp.exp(prior_decay - enter_max)
    carry_memory = (
        from_prior[:, None, None] * prior_memory + from_first[:, None, None] * first_memory
    )
    carry_norm = from_prior[:, None] * prior_norm + from_first[:, None] * first_norm
    query_scale = KEY_DIM ** (-0.5)
    row_ids = lax.iota(jnp.int32, row_count)
    causal = row_ids[:, None] >= row_ids[None, :]
    cum_heads = cumulative.T
    log_gap = cum_heads[:, :, None] - cum_heads[:, None, :] + in_pre.T[:, None, :]
    log_gap = jnp.where(causal[None], log_gap, -jnp.inf)
    inter_log = cum_heads + enter_max[:, None]
    row_max = jnp.maximum(inter_log, jnp.max(log_gap, axis=2))
    raw_scores = (
        jnp.einsum("thd,shd->hts", query_rows, key_rows, preferred_element_type=jnp.float32)
        * query_scale
    )
    mixing = raw_scores * jnp.exp(log_gap - row_max[:, :, None])
    carried = jnp.exp(inter_log - row_max).T
    scaled_query = query_rows.astype(jnp.float32) * query_scale
    from_values = jnp.einsum(
        "hts,shv->thv", mixing.astype(jnp.bfloat16), value_rows, preferred_element_type=jnp.float32
    )
    from_memory = jnp.einsum("thd,hdv->thv", scaled_query, carry_memory, precision=highest)
    from_norm = jnp.einsum("thd,hd->th", scaled_query, carry_norm, precision=highest)
    numerator = from_values + carried[:, :, None] * from_memory
    denominator = jnp.sum(mixing, axis=2).T + carried * from_norm
    memory_out = numerator / jnp.maximum(jnp.abs(denominator), 1.0)[:, :, None]
    local_squares = jnp.sum(memory_out * memory_out, axis=(1, 2))
    row_total = lax.psum(local_squares, "tp")
    row_scale = lax.rsqrt(row_total / V_WIDTH + epsilon)
    heads_out = memory_out * row_scale[:, None, None]
    heads_out = heads_out.reshape(row_count, value_width).astype(jnp.bfloat16)
    padded = jnp.concatenate([before_rows, product], axis=0).astype(jnp.float32)
    filtered = taps_here[0][None, :] * padded[0:row_count]
    for tap_index in range(1, TAPS):
        filtered = (
            filtered + taps_here[tap_index][None, :] * padded[tap_index : tap_index + row_count]
        )
    conv_branch = (conv_gate * filtered).astype(jnp.bfloat16)
    return lax.psum_scatter(
        (
            jnp.dot(heads_out, w_out_memory, preferred_element_type=jnp.float32)
            + jnp.dot(conv_branch, w_out_conv, preferred_element_type=jnp.float32)
        ).astype(jnp.bfloat16),
        "tp",
        scatter_dimension=0,
        tiled=True,
    )


def solution(mesh):
    in_specs = (
        P(("sp", "tp"), None),
        P(),
        P(None, "tp"),
        P(None, "tp"),
        P(None, "tp"),
        P(),
        P(),
        P(),
        P("sp", "tp"),
        P(None, "tp"),
        P(None, "tp"),
        P(None, "tp"),
        P(),
        P("tp", None, None),
        P("tp", None),
        P("tp", None),
        P("tp", None),
    )
    out_specs = P(("sp", "tp"), None)
    return jax.shard_map(
        per_device, mesh=mesh, in_specs=in_specs, out_specs=out_specs, check_vma=False
    )
```

profile of v0, /device:TPU:0, one launch (start us, length us, event | category | flops | bytes accessed | tf_op | source)
XLA Modules:
  0.0 204.8 jit_solution(13238146320118617703)
XLA Ops:
  6.5 1.5 fusion.13
  8.1 2.3 %fusion.15 = bf16[192,2048]{1,0:T(8,128)(2,1)} fusion(bf16[192,2048]{1,0:T(8,128)(2,1)} %param.19, f32[2048]{0:T(1024)} %param.20, f32[192]{0:T(256)S(1)} %add_rsqrt_fusion.1), kind=kLoop, calls=%fused_computation.26 | loop fusion | flops 1572864 | bytes 1581824 | tf_op jit(solution)/shard_map/convert_element_type | solution.py:84
  10.4 0.1 dynamic_slice.28
  10.5 31.2 %all-gather.6.cloned.1.call-done = bf16[768,2048]{1,0:T(8,128)(2,1)} async-done(((bf16[192,2048]{1,0:T(8,128)(2,1)}), bf16[768,2048]{1,0:T(8,128)(2,1)}) %all-gather.6.cloned.1.call-update) | async-done | bytes 3145744 | tf_op jit(solution)/shard_map/all_gather | solution.py:85
  41.8 2.8 %fusion.43 = f32[2,768]{1,0:T(2,128)S(1)} fusion(f32[768,2]{0,1:T(2,128)S(1)} %copy-done.11, bf16[768,2048]{1,0:T(8,128)(2,1)} %all-gather.6.cloned.1.call-done, bf16[2048,8]{0,1:T(8,128)(2,1)} %param.25, s32[]{:T(128)S(6)} %select_n.26, f32[2]{0:T(128)S(1)} %dynamic_slice.28), kind=kOutput, calls=%fused_computation.74 | convolution fusion | flops 6306816 | bytes 3166220 | tf_op jit(solution)/shard_map/dot_general | solution.py:87
  44.6 0.6 reduce-window.6
  45.2 0.2 slice_reduce_fusion
  45.4 0.2 reduce-window.9
  45.5 0.1 add_bitcast_fusion
  45.6 0.2 slice_reduce_fusion.1
  45.8 3.1 %fusion.56 = (f32[2]{0:T(128)S(1)}, f32[768,2]{0,1:T(2,128)S(1)}, f32[768,2]{0,1:T(2,128)S(1)}) fusion(f32[2,768]{1,0:T(2,128)S(1)} %bitcast.127, f32[2]{0:T(128)S(1)} %slice_reduce_fusion.1, bf16[768,2048]{1,0:T(8,128)(2,1)} %all-gather.6.cloned.1.call-done, bf16[2048,8]{0,1:T(8,128)(2,1)} %param.24, s32[]{:T(128)S(6)} %select_n.26), kind=kOutput, calls=%fused_computation.97 | convolution fusion | flops 6296062 | bytes 3172372 | tf_op jit(solution)/shard_map/dot_general | solution.py:87
  48.9 0.1 subtract_exponential_fusion.2
  49.0 0.3 copy-done.13
  49.3 1.9 convolution_convert_fusion.3
  51.2 1.1 fusion.24
  52.4 0.7 copy-done.5
  53.1 1.1 fusion.29
  54.3 0.6 dynamic-slice
  55.4 0.9 constant_dynamic-slice_fusion.2
  56.3 0.2 iota_compare_fusion
  56.5 0.2 dynamic-update-slice
  56.7 20.5 %all-gather.2 = f32[8,1,2]{2,1,0:T(1,128)S(1)} all-gather(f32[1,1,2]{2,1,0:T(1,128)S(1)} %bitcast.139), channel_id=1, replica_groups=mesh['sp'=8,'tp'=4] {'sp'}, dimensions={0}, use_global_device_ids=true | all-gather | bytes 72 | tf_op jit(solution)/shard_map/all_gather | solution.py:25
  77.2 17.7 %all-reduce = f32[16]{0:T(128)S(1)} all-reduce(f32[16]{0:T(128)S(1)} %dynamic-update-slice), channel_id=2, replica_groups=mesh['sp'=8,'tp'=4] {'sp'}, use_global_device_ids=true, to_apply=%add | all-reduce | flops 16 | bytes 128
  95.0 0.1 reshape.111
  95.0 3.3 %convolution_convert_fusion.5 = bf16[768,256]{0,1:T(8,128)(2,1)S(1)} fusion(bf16[768,2048]{1,0:T(8,128)(2,1)} %all-gather.6.cloned.1.call-done, bf16[2048,256]{1,0:T(8,128)(2,1)} %param.21), kind=kOutput, calls=%fused_computation.45 | convolution fusion | flops 805502976 | bytes 4587520 | tf_op jit(solution)/shard_map/dot_general | solution.py:87
  98.3 0.2 copy.40
  98.6 4.5 %convolution_convert_fusion = bf16[768,512]{1,0:T(8,128)(2,1)S(1)} fusion(bf16[768,2048]{1,0:T(8,128)(2,1)} %all-gather.6.cloned.1.call-done, bf16[2048,512]{1,0:T(8,128)(2,1)} %param.30), kind=kOutput, calls=%fused_computation.40 | convolution fusion | flops 1611005952 | bytes 6029312 | tf_op jit(solution)/shard_map/dot_general | solution.py:87
  103.1 1.8 convolution_convert_fusion.1
  104.9 0.2 multiply_convert_fusion
  105.1 3.9 %collective-permute-start = (bf16[2,512]{1,0:T(2,128)(2,1)S(1)}, bf16[2,512]{1,0:T(2,128)(2,1)S(1)}, u32[]{:S(2)}, u32[]{:S(2)}) collective-permute-start(bf16[2,512]{1,0:T(2,128)(2,1)S(1)} %slice.42), channel_id=1, source_target_pairs={{0,4},{4,8},{8,12},{12,16},{16,20},{20,24},{24,28},{1,5},{5,9},{9,... | collective-permute-start | bytes 6152 | tf_op jit(solution)/shard_map/ppermute | solution.py:20
  109.1 2.7 %convolution_convert_fusion.2 = bf16[768,512]{1,0:T(8,128)(2,1)} fusion(bf16[768,2048]{1,0:T(8,128)(2,1)S(1)} %copy-done.2, bf16[2048,512]{1,0:T(8,128)(2,1)S(1)} %copy-done.15), kind=kOutput, calls=%fused_computation.42 | convolution fusion | flops 1611005952 | bytes 6029312 | tf_op jit(solution)/shard_map/dot_general | solution.py:87
  111.8 0.9 fusion.7
  112.7 16.5 %all_gather.31 = f32[8,2,128]{2,1,0:T(2,128)S(1)} all-gather(f32[1,2,128]{2,1,0:T(2,128)S(1)} %bitcast.142), channel_id=1, replica_groups=mesh['sp'=8,'tp'=4] {'sp'}, dimensions={0}, use_global_device_ids=true | all-gather | bytes 9216 | tf_op jit(solution)/shard_map/all_gather | solution.py:25
  129.2 1.4 maximum_convert_fusion
  130.7 0.1 add_maximum_fusion
  130.8 3.4 %fusion.8 = (f32[2,768]{1,0:T(2,128)S(1)}, f32[2,768,768]{1,2,0:T(8,128)S(1)}) fusion(f32[2,768]{1,0:T(2,128)S(1)} %add_maximum_fusion, f32[2,768]{1,0:T(2,128)S(1)} %bitcast.132, f32[2,768]{1,0:T(2,128)S(1)} %bitcast.129, pred[768,768]{0,1:T(8,128)(4,1)S(1)} %iota_compare_fusion, bf16[768,2,128]{0,2,1:T(8,128)(2,1)} %bitcast.126, ...), kind=kOutput, calls=%fused_computation.17 | convolution fusion | flops 310245888 | bytes 6119424 | tf_op jit(solution)/shard_map/thd,shd->hts/dot_general | solution.py:162
  134.2 2.2 %fusion.10 = f32[2,256,768]{2,1,0:T(8,128)S(1)} fusion(bf16[768,2,256]{0,2,1:T(8,128)(2,1)S(1)} %bitcast.124, f32[2,768,768]{1,2,0:T(8,128)S(1)} %get-tuple-element.131, f32[2,768]{1,0:T(2,128)S(1)} %add_maximum_fusion, f32[2,768]{1,0:T(2,128)S(1)} %bitcast.133, f32[2,768]{1,0:T(2,128)S(1)} %bitcast.130, pred[768,768]{0,1:T(8,128)(4,1)S(1)} %iota_compare_fusion), kind=kOutput, calls=%fused_computation.20 | convolution fusion | flops 612237312 | bytes 7686144 | tf_op jit(solution)/shard_map/hts,shv->thv/dot_general | solution.py:168
  136.4 0.1 multiply_add_fusion
  136.5 0.7 fusion.28
  137.2 0.1 fusion.46
  137.4 2.9 %multiply_reduce_fusion = (f32[768]{0:T(1024)S(1)}, f32[768,2,256]{0,2,1:T(8,128)}) fusion(f32[768,2]{0,1:T(2,128)S(1)} %get-tuple-element.117, bf16[768,2,128]{2,0,1:T(8,128)(2,1)S(1)} %copy.40, f32[2,128,256]{2,1,0:T(8,128)S(1)} %copy-done.16, f32[2,128,256]{2,1,0:T(8,128)S(1)} %get-tuple-element.63, f32[2]{0:T(128)S(1)} %subtract_exponential_fusion.3, ...), kind=kOutput, calls=%fused_computation.39 | convolution fusion | flops 606534912 | bytes 4078608 | tf_op jit(solution)/shard_map/thd,hdv->thv/dot_general | solution.py:171
  140.3 5.9 %psum.7 = f32[768]{0:T(1024)S(1)} all-reduce(f32[768]{0:T(1024)S(1)} %get-tuple-element.132), channel_id=1, replica_groups=mesh['sp'=8,'tp'=4] {'tp'}, use_global_device_ids=true, to_apply=%region_10.11 | all-reduce | flops 768 | bytes 6144 | tf_op jit(solution)/shard_map/psum | solution.py:177
  146.1 1.5 multiply_convert_fusion.1
  147.7 1.9 fusion.57
  149.6 0.2 copy-done.4
  149.8 0.2 copy-done.9
  149.9 3.8 %add_convert_fusion = bf16[768,2048]{1,0:T(8,128)(2,1)} fusion(f32[768,2048]{1,0:T(8,128)S(1)} %fusion.57, bf16[512,2048]{1,0:T(8,128)(2,1)S(1)} %copy-done.4, f32[770,512]{1,0:T(8,128)S(1)} %copy-done.3, bf16[768,512]{1,0:T(8,128)(2,1)S(1)} %copy-done.9, f32[512]{0:T(512)S(1)} %bitcast.137, f32[512]{0:T(512)S(1)} %bitcast.136, f32[512]{0:T(512)S(1)} %bitcast.135), kind=kOutput, calls=%fused_computation.13 | convolution fusion | flops 1616904192 | bytes 17045504 | tf_op jit(solution)/shard_map/dot_general | solution.py:191
  153.7 44.5 %reduce-scatter.2.cloned.1.call-done = bf16[192,2048]{1,0:T(8,128)(2,1)} async-done(((bf16[768,2048]{1,0:T(8,128)(2,1)}), bf16[192,2048]{1,0:T(8,128)(2,1)}) %reduce-scatter.2.cloned.1.call-update) | async-done | bytes 786448 | tf_op jit(solution)/shard_map/reduce_scatter | solution.py:188
  (56 shorter events, 0.3 us)
Async XLA Ops:
  6.5 141.1 %copy-start = (bf16[512,2048]{1,0:T(8,128)(2,1)S(1)}, bf16[512,2048]{1,0:T(8,128)(2,1)}, u32[]{:S(2)}) copy-start(bf16[512,2048]{1,0:T(8,128)(2,1)} %param.34) | copy-start | bytes 6291460
  6.5 3.9 %copy-start.17 = (f32[8]{0:T(128)S(1)}, f32[8]{0:T(128)}, u32[]{:S(2)}) copy-start(f32[8]{0:T(128)} %param.26) | copy-start | bytes 100
  6.5 35.2 %copy-start.11 = (f32[768,2]{0,1:T(2,128)S(1)}, f32[768,2]{0,1:T(2,128)}, u32[]{:S(2)}) copy-start(f32[768,2]{0,1:T(2,128)} %param.27) | copy-start | bytes 18436
  6.5 35.2 %all-gather.6.cloned.1.call-start = ((), (), s32[]{:S(2)}) async-start(), calls=%async_computation.1 | async-start | bytes 3932160 | tf_op jit(solution)/shard_map/all_gather | solution.py:85
  10.4 120.2 %all-gather.8.cloned.1.call-start = ((), (), s32[]{:S(2)}) async-start(), calls=%async_computation.3 | async-start | bytes 2359296 | tf_op jit(solution)/shard_map/all_gather | solution.py:25
  45.8 3.2 %copy-start.1 = (bf16[768,2048]{1,0:T(8,128)(2,1)S(1)}, bf16[768,2048]{1,0:T(8,128)(2,1)}, u32[]{:S(2)}) copy-start(bf16[768,2048]{1,0:T(8,128)(2,1)} %all-gather.6.cloned.1.call-done) | copy-start | bytes 9437188
  45.8 3.5 %copy-start.13 = (bf16[2048,512]{1,0:T(8,128)(2,1)S(1)}, bf16[2048,512]{1,0:T(8,128)(2,1)}, u32[]{:S(2)}) copy-start(bf16[2048,512]{1,0:T(8,128)(2,1)} %param.23) | copy-start | bytes 6291460
  49.3 1.9 copy-start.6
  51.2 1.1 copy-start.7
  51.2 3.1 %copy-start.18 = (u32[32]{0:T(128)S(1)}, u32[32]{0:T(128)}, u32[]{:S(2)}) copy-start(u32[32]{0:T(128)} %constant.70) | copy-start | bytes 388
  52.3 0.8 copy-start.5
  54.2 144.0 %reduce-scatter.2.cloned.1.call-start = ((), (), s32[]{:S(2)}) async-start(), calls=%async_computation.2 | async-start | bytes 3932160 | tf_op jit(solution)/shard_map/reduce_scatter | solution.py:188
  98.3 4.7 %copy-start.10 = (bf16[768,256]{0,1:T(8,128)(2,1)}, bf16[768,256]{0,1:T(8,128)(2,1)S(1)}, u32[]{:S(2)}) copy-start(bf16[768,256]{0,1:T(8,128)(2,1)S(1)} %convolution_convert_fusion.5) | copy-start | bytes 1179652
  98.5 4.5 %copy-start.2 = (bf16[768,2048]{1,0:T(8,128)(2,1)S(1)}, bf16[768,2048]{1,0:T(8,128)(2,1)}, u32[]{:S(2)}) copy-start(bf16[768,2048]{1,0:T(8,128)(2,1)} %all-gather.6.cloned.1.call-done) | copy-start | bytes 9437188
  98.5 4.5 %copy-start.14 = (bf16[2048,512]{1,0:T(8,128)(2,1)S(1)}, bf16[2048,512]{1,0:T(8,128)(2,1)}, u32[]{:S(2)}) copy-start(bf16[2048,512]{1,0:T(8,128)(2,1)} %param.29) | copy-start | bytes 6291460
  104.9 4.2 %copy-start.15 = (bf16[2048,512]{1,0:T(8,128)(2,1)S(1)}, bf16[2048,512]{1,0:T(8,128)(2,1)}, u32[]{:S(2)}) copy-start(bf16[2048,512]{1,0:T(8,128)(2,1)} %param.28) | copy-start | bytes 6291460
  105.1 24.1 %collective-permute-start = (bf16[2,512]{1,0:T(2,128)(2,1)S(1)}, bf16[2,512]{1,0:T(2,128)(2,1)S(1)}, u32[]{:S(2)}, u32[]{:S(2)}) collective-permute-start(bf16[2,512]{1,0:T(2,128)(2,1)S(1)} %slice.42), channel_id=1, source_target_pairs={{0,4},{4,8},{8,12},{12,16},{16,20},{20,24},{24,28},{1,5},{5,9},{9,... | collective-permute-start | bytes 6152 | tf_op jit(solution)/shard_map/ppermute | solution.py:20
  130.8 3.4 %copy-start.8 = (bf16[768,512]{0,1:T(8,128)(2,1)S(1)}, bf16[768,512]{0,1:T(8,128)(2,1)}, u32[]{:S(2)}) copy-start(bf16[768,512]{0,1:T(8,128)(2,1)} %copy-done.7) | copy-start | bytes 2359300
  134.2 2.2 %copy-start.12 = (f32[2,128]{1,0:T(2,128)S(1)}, f32[2,128]{1,0:T(2,128)}, u32[]{:S(2)}) copy-start(f32[2,128]{1,0:T(2,128)} %param.33) | copy-start | bytes 3076
  134.2 3.1 %copy-start.16 = (f32[2,128,256]{2,1,0:T(8,128)S(1)}, f32[2,128,256]{2,1,0:T(8,128)}, u32[]{:S(2)}) copy-start(f32[2,128,256]{2,1,0:T(8,128)} %param.32) | copy-start | bytes 786436
  147.7 1.9 copy-start.3
  147.7 2.1 %copy-start.4 = (bf16[512,2048]{1,0:T(8,128)(2,1)S(1)}, bf16[512,2048]{1,0:T(8,128)(2,1)}, u32[]{:S(2)}) copy-start(bf16[512,2048]{1,0:T(8,128)(2,1)} %param.35) | copy-start | bytes 6291460
  147.7 2.2 %copy-start.9 = (bf16[768,512]{1,0:T(8,128)(2,1)S(1)}, bf16[768,512]{1,0:T(8,128)(2,1)}, u32[]{:S(2)}) copy-start(bf16[768,512]{1,0:T(8,128)(2,1)} %convolution_convert_fusion.2) | copy-start | bytes 2359300
Sparse Core Ops, SparseCore 0:
  10.5 31.2 all-gather.5
  54.3 48.8 all-gather.7
  153.8 44.3 reduce-scatter.1
where the time goes:
time: 205 us
  waiting for transfers between devices  75.8 us (37%)
  blocking collectives  60.6 us (30%)
  matrix products  37.1 us (18%)
  between operations  14.1 us (7%)
  other arithmetic  9.26 us (5%)
  starting transfers between devices  4.02 us (2%)
  local copies, waits for them, and re-layouts  3.93 us (2%)
    reduce_scatter x1, waiting for transfers between devices, per_device(): lax.psum_scatter((jnp.dot(heads_out, w_out_memory, preferred_element_type...  44.5 us
    all_gather x2, blocking collectives, entering(): gathered = jax.tree.map(lambda a: lax.all_gather(a, axis), part)  37 us
    all_gather x1, waiting for transfers between devices, per_device(): sub_rows = lax.all_gather(normed, 'tp', axis=0, tiled=True)  31.2 us
    dot_general x8, matrix products, per_device(): jnp.dot(sub_rows, weight, preferred_element_type=jnp.float32)  21.1 us
    unnamed x1, blocking collectives  17.7 us
    psum x1, blocking collectives, per_device(): row_total = lax.psum(local_squares, 'tp')  5.88 us
  transfers between devices with their start and end apart: 4, of which 2 were waited for; matrix products, arithmetic and copies ran while one was open for 8% of the time, Pallas kernels for 0%

commit v1 on v0

v1 whole, which is shorter than its diff:
```python
import functools

import jax
import jax.numpy as jnp
from jax import lax
from jax.experimental import pallas as pl
from jax.experimental.pallas import tpu as pltpu
from jax.sharding import PartitionSpec as P

KEY_DIM = 128
VALUE_DIM = 256
TAPS = 3
EPS = 1e-06
NEG = -1e30
MESH = pl.DeviceIdType.MESH
F32 = jnp.float32
BF16 = jnp.bfloat16
AG_CHUNKS = 3
RS_CHUNKS = 4


def mm(a, b):
    return lax.dot_general(a, b, (((1,), (0,)), ((), ())), preferred_element_type=F32)


def mm_t(a, b):
    return lax.dot_general(a, b, (((1,), (1,)), ((), ())), preferred_element_type=F32)


def scan_steps(n):
    steps, d = [], 1
    while d < n:
        steps.append(d)
        d *= 2
    return steps


def kernel(
    n_sp, n_tp, heads, channels, width,
    tokens, gain, wk, wv, wg, wq, wcg, wcl, wcr, bias, extra, taps, first_mem, first_norm,
    wom, woc, out,
    W, WO, XG, PJ, G, COL, NUM, DEN, HC, PROD, halo_out, halo_in,
    A_mem, E_mem, sm_out, sm_in, mem_out_b, mem_in_b, sq_out, sq_in,
    PS, DR, YS, YR,
    w_sem, ag_d, ag_ys, ag_yr, ag_fs, ag_fr, st_s, st_r, hl_s, sq_s, sq_r,
    rd_s, rd_r, ry_s, ry_r,
):
    sp = lax.axis_index("sp")
    tp = lax.axis_index("tp")
    core = lax.rem(tp, 2)
    y = tp // 2
    n_y = n_tp // 2
    partner = tp + 1 - 2 * core
    R, D = tokens.shape
    T = R * n_tp
    qk, vw = heads * KEY_DIM, heads * VALUE_DIM
    o_v, o_g = qk, qk + vw
    o_q = o_g + 128
    o_c = o_q + qk
    total = o_c + 3 * channels
    steps = scan_steps(n_sp)

    srcs = [(wk, 0, qk), (wv, o_v, vw), (wg, o_g, 128), (wq, o_q, qk), (wcg, o_c, channels),
            (wcl, o_c + channels, channels), (wcr, o_c + 2 * channels, channels)]
    w_copies = [
        pltpu.make_async_copy(s, W.at[:, pl.ds(o, n)], w_sem.at[i])
        for i, (s, o, n) in enumerate(srcs)
    ]
    w_copies.append(pltpu.make_async_copy(wom, WO.at[pl.ds(0, vw), :], w_sem.at[7]))
    w_copies.append(pltpu.make_async_copy(woc, WO.at[pl.ds(vw, channels), :], w_sem.at[8]))
    for c in w_copies:
        c.start()

    def rows_of(block, count=1, first=0, n=None):
        n = R * count if n is None else n
        return pl.ds(pl.multiple_of(block * R + first, 16), n)

    x = tokens[...].astype(F32)
    scale = lax.rsqrt(jnp.mean(x * x, axis=1, keepdims=True) + EPS)
    XG[rows_of(tp), :] = (x * scale * gain[...]).astype(BF16)

    def remote(src, dst, ss, rs, to_tp=None, to_sp=None):
        return pltpu.make_async_remote_copy(
            src_ref=src, dst_ref=dst, send_sem=ss, recv_sem=rs,
            device_id=(sp if to_sp is None else to_sp, tp if to_tp is None else to_tp),
            device_id_type=MESH,
        )

    offsets = sorted({d % n_sp for d in steps} | {(n_sp - d) % n_sp for d in steps})
    barrier = pltpu.get_barrier_semaphore()
    for k in range(1, n_tp):
        pl.semaphore_signal(barrier, inc=1, device_id=(sp, lax.rem(tp + k, n_tp)), device_id_type=MESH)
    for k in offsets:
        pl.semaphore_signal(barrier, inc=1, device_id=(lax.rem(sp + k, n_sp), tp), device_id_type=MESH)
    pl.semaphore_wait(barrier, n_tp - 1 + len(offsets))

    sends = []
    piece = R // AG_CHUNKS
    for c in range(AG_CHUNKS):
        for k in range(1, n_y):
            r = rows_of(tp, 1, c * piece, piece)
            cp = remote(XG.at[r, :], XG.at[r, :], ag_ys.at[k - 1, c], ag_yr.at[k - 1, c],
                        to_tp=lax.rem(y + k, n_y) * 2 + core)
            cp.start()
            sends.append(cp)
    own = remote(XG.at[rows_of(tp), :], XG.at[rows_of(tp), :], ag_d.at[0], ag_d.at[1], to_tp=partner)
    own.start()

    tn = 256 if (o_g % 256 == 0 and qk % 256 == 0) else 128

    def project(block, first, last):
        rr = rows_of(block, 2)

        def one(j, _):
            cols = pl.ds(pl.multiple_of(first + j * tn, 128), tn)
            PJ[rr, cols] = mm(XG[rr, :], W[:, cols]).astype(BF16)
            return 0

        lax.fori_loop(0, (last - first) // tn, one, 0)

    def project_gates(block):
        rr = rows_of(block, 2)
        G[rr, :] = mm(XG[rr, :], W[:, o_g:o_g + 128])

    own.wait_recv()
    for c in w_copies[:3]:
        c.wait()
    project(2 * y, 0, o_g)
    project_gates(2 * y)
    for c in w_copies[3:7]:
        c.wait()
    project(2 * y, o_q, total)
    fwd = []
    for c in range(AG_CHUNKS):
        for k in range(1, n_y):
            src = lax.rem(y + n_y - k, n_y) * 2
            r = rows_of(src + core, 1, c * piece, piece)
            remote(XG.at[r, :], XG.at[r, :], ag_ys.at[k - 1, c], ag_yr.at[k - 1, c], to_tp=partner).wait_recv()
            cp = remote(XG.at[r, :], XG.at[r, :], ag_fs.at[k - 1, c], ag_fr.at[k - 1, c], to_tp=partner)
            cp.start()
            sends.append(cp)
    for c in range(AG_CHUNKS):
        for k in range(1, n_y):
            src = lax.rem(y + n_y - k, n_y) * 2
            r = rows_of(src + 1 - core, 1, c * piece, piece)
            remote(XG.at[r, :], XG.at[r, :], ag_fs.at[k - 1, c], ag_fr.at[k - 1, c], to_tp=partner).wait_recv()
    others = [lax.rem(y + k, n_y) * 2 for k in range(1, n_y)]
    for b in others:
        project(b, 0, o_g)
        project_gates(b)

    n_heads = bias.shape[0]
    gt = G[...].T
    in_all, forget_all = gt[0:n_heads], gt[n_heads:2 * n_heads]
    sub = lax.broadcasted_iota(jnp.int32, (n_heads, T), 0)
    sub8 = lax.broadcasted_iota(jnp.int32, (8, T), 0)
    lane = lax.broadcasted_iota(jnp.int32, (8, T), 1)
    in_pre = jnp.zeros((8, T), F32)
    log_f = jnp.zeros((8, T), F32)
    for h in range(heads):
        head = tp * heads + h
        row_i = jnp.sum(jnp.where(sub == head, in_all, 0.0), axis=0, keepdims=True)
        row_f = jnp.sum(jnp.where(sub == head, forget_all, 0.0), axis=0, keepdims=True) + bias[head]
        row_f = jnp.minimum(row_f, 0.0) - jnp.log1p(jnp.exp(-jnp.abs(row_f))) + extra[h:h + 1, :]
        in_pre = jnp.where(sub8 == h, row_i, in_pre)
        log_f = jnp.where(sub8 == h, row_f, log_f)
    cum = log_f
    for d in scan_steps(T):
        cum = cum + jnp.where(lane >= d, pltpu.roll(cum, d, 1), 0.0)
    gap = in_pre - cum
    run = gap
    for d in scan_steps(T):
        run = jnp.maximum(run, jnp.where(lane >= d, pltpu.roll(run, d, 1), run))
    decay = cum[:, T - 1:T]
    gmax = run[:, T - 1:T]
    COL[...] = jnp.concatenate(
        [gap, run, jnp.exp(gap - gmax), jnp.zeros((104, T), F32)], axis=0).T
    ones = jnp.ones((1, 128), F32)

    sm = jnp.zeros((8, 128), F32)
    s8 = lax.broadcasted_iota(jnp.int32, (8, 128), 0)
    for h in range(heads):
        keyed = PJ[:, h * KEY_DIM:(h + 1) * KEY_DIM].astype(F32) * COL[:, 16 + h:17 + h]
        norm = jnp.sum(keyed, axis=0, keepdims=True)
        mem = mm(keyed.T.astype(BF16), PJ[:, o_v + h * VALUE_DIM:o_v + (h + 1) * VALUE_DIM])
        A_mem[h] = mem
        mem_out_b[0, h] = mem.astype(BF16)
        sm = jnp.where(s8 == h, norm, sm)
        sm = jnp.where(s8 == heads + h, decay[h:h + 1] * ones, sm)
        sm = jnp.where(s8 == 2 * heads + h, (decay[h:h + 1] + gmax[h:h + 1]) * ones, sm)
    E_mem[...] = jnp.zeros_like(E_mem)
    sm_out[0] = sm

    def state_copies(i, forward):
        d = steps[i]
        to = lax.rem(sp + d, n_sp)
        return (remote(mem_out_b.at[i], mem_in_b.at[i], st_s.at[i, 0], st_r.at[i, 0], to_sp=to),
                remote(sm_out.at[i], sm_in.at[i], st_s.at[i, 1], st_r.at[i, 1], to_sp=to))

    def state_send(i):
        for cp in state_copies(i, True):
            cp.start()
            sends.append(cp)

    def part(s, j, h):
        return s[j * heads + h:j * heads + h + 1]

    def join(valid, early, early_mem, late, late_mem, h):
        n_e, d_e, m_e = part(early, 0, h), part(early, 1, h), part(early, 2, h)
        n_l, d_l, m_l = part(late, 0, h), part(late, 1, h), part(late, 2, h)
        d_e = jnp.where(valid, d_e, 0.0)
        m_e = jnp.where(valid, m_e, NEG)
        top = jnp.maximum(m_e + d_l, m_l)
        s_e = jnp.where(valid, jnp.exp(m_e + d_l - top), 0.0)
        s_l = jnp.exp(m_l - top)
        return (s_e * n_e + s_l * n_l, d_e + d_l, top,
                s_e[:, 0:1] * early_mem + s_l[:, 0:1] * late_mem)

    state = {"a": sm, "e": jnp.where(s8 >= 2 * heads, NEG, 0.0)}

    def state_step(i):
        for cp in state_copies(i, False):
            cp.wait_recv()
        valid = sp >= steps[i]
        got = sm_in[i]
        last = i + 1 == len(steps)
        for which, ref in (("e", E_mem), ("a", A_mem)):
            if which == "a" and last:
                continue
            new = jnp.zeros((8, 128), F32)
            for h in range(heads):
                n_j, d_j, m_j, mem = join(valid, got, mem_in_b[i, h].astype(F32), state[which], ref[h], h)
                ref[h] = mem
                if which == "a":
                    mem_out_b[i + 1, h] = mem.astype(BF16)
                new = jnp.where(s8 == h, n_j, new)
                new = jnp.where(s8 == heads + h, d_j, new)
                new = jnp.where(s8 == 2 * heads + h, m_j, new)
            state[which] = new
            if which == "a":
                sm_out[i + 1] = new
        if not last:
            state_send(i + 1)

    state_send(0)
    for b in others:
        project(b, o_q, total)

    rb = 256 if T % 256 == 0 else R
    for r0 in range(0, T, rb):
        left = PJ[r0:r0 + rb, o_c + channels:o_c + 2 * channels].astype(F32)
        right = PJ[r0:r0 + rb, o_c + 2 * channels:o_c + 3 * channels].astype(F32)
        prod = (left * right).astype(BF16)
        PROD[8 + r0:8 + r0 + rb, :] = prod.astype(F32)
        if r0 + rb == T:
            halo_out[...] = prod[rb - 16:rb]
    halo = remote(halo_out, halo_in, hl_s.at[0], hl_s.at[1], to_sp=lax.rem(sp + 1, n_sp))
    halo.start()
    sends.append(halo)

    q_scale = KEY_DIM ** -0.5

    def attend(h, r0):
        e = r0 + rb
        q = PJ[r0:e, o_q + h * KEY_DIM:o_q + (h + 1) * KEY_DIM]
        k = PJ[0:e, h * KEY_DIM:(h + 1) * KEY_DIM]
        v = PJ[0:e, o_v + h * VALUE_DIM:o_v + (h + 1) * VALUE_DIM]
        s = mm_t(q, k) * q_scale
        ti = lax.broadcasted_iota(jnp.int32, (rb, e), 0) + r0
        si = lax.broadcasted_iota(jnp.int32, (rb, e), 1)
        w = jnp.where(ti >= si, gap[h:h + 1, 0:e] - COL[r0:e, 8 + h:9 + h], NEG)
        mix = s * jnp.exp(w)
        DEN[h, r0:e, :] = jnp.broadcast_to(jnp.sum(mix, axis=1, keepdims=True), (rb, 128))
        NUM[r0:e, h * VALUE_DIM:(h + 1) * VALUE_DIM] = mm(mix.astype(BF16), v)

    work = [functools.partial(attend, h, r0) for h in range(heads) for r0 in range(0, T, rb)]

    def conv_finish():
        halo.wait_recv()
        before = halo_in[...].astype(F32)[8:16]
        PROD[0:8, :] = jnp.where(sp > 0, before, 0.0)
        tap = taps[:, pl.ds(pl.multiple_of(tp * channels, 128), channels)]
        for r0 in range(0, T, rb):
            f = tap[0:1] * PROD[6 + r0:6 + r0 + rb, :]
            f = f + tap[1:2] * PROD[7 + r0:7 + r0 + rb, :]
            f = f + tap[2:3] * PROD[8 + r0:8 + r0 + rb, :]
            gate = PJ[r0:r0 + rb, o_c:o_c + channels].astype(F32)
            HC[r0:r0 + rb, vw:] = (gate * f).astype(BF16)

    work.append(conv_finish)
    share = -(-len(work) // len(steps))
    for i in range(len(steps)):
        state_step(i)
        if i + 1 < len(steps):
            for w_ in work[:share]:
                w_()
            work = work[share:]
        elif work:
            for w_ in work:
                w_()

    e_s = state["e"]
    sq = [jnp.zeros((rb, 1), F32) for _ in range(T // rb)]
    for h in range(heads):
        n_e, d_e, m_e = part(e_s, 0, h), part(e_s, 1, h), part(e_s, 2, h)
        cmax = jnp.maximum(m_e, d_e)
        s_p, s_f = jnp.exp(m_e - cmax), jnp.exp(d_e - cmax)
        c_mem = s_p[:, 0:1] * E_mem[h] + s_f[:, 0:1] * first_mem[h]
        c_norm = s_p * n_e + s_f * first_norm[h:h + 1, :]
        hi = c_mem.astype(BF16)
        lo = (c_mem - hi.astype(F32)).astype(BF16)
        for b, r0 in enumerate(range(0, T, rb)):
            e = r0 + rb
            q = PJ[r0:e, o_q + h * KEY_DIM:o_q + (h + 1) * KEY_DIM]
            fm = mm(q, hi) + mm(q, lo)
            fn = jnp.sum(q.astype(F32) * c_norm, axis=1, keepdims=True)
            m0 = COL[r0:e, 8 + h:9 + h]
            m = jnp.maximum(m0, cmax[:, 0:1])
            k0 = jnp.exp(m0 - m)
            k1 = jnp.exp(cmax[:, 0:1] - m) * q_scale
            den = k0 * DEN[h, r0:e, 0:1] + k1 * fn
            inv = 1.0 / jnp.maximum(jnp.abs(den), 1.0)
            cols = slice(h * VALUE_DIM, (h + 1) * VALUE_DIM)
            mo = (k0 * NUM[r0:e, cols] + k1 * fm) * inv
            NUM[r0:e, cols] = mo
            sq[b] = sq[b] + jnp.sum(mo * mo, axis=1, keepdims=True)
    sq_col = jnp.concatenate([jnp.broadcast_to(s, (rb, 128)) for s in sq], axis=0)
    mine = sq_col.T[0:8]
    sq_out[...] = mine
    for k in range(1, n_tp):
        cp = remote(sq_out, sq_in.at[k - 1], sq_s.at[k - 1], sq_r.at[k - 1], to_tp=lax.rem(tp + k, n_tp))
        cp.start()
        sends.append(cp)
    tot = mine
    for k in range(1, n_tp):
        remote(sq_out, sq_in.at[k - 1], sq_s.at[k - 1], sq_r.at[k - 1], to_tp=partner).wait_recv()
        tot = tot + sq_in[k - 1]
    r_scale = lax.rsqrt(tot / float(width) + EPS)
    COL[...] = jnp.concatenate([r_scale] * 16, axis=0).T
    for r0 in range(0, T, rb):
        HC[r0:r0 + rb, 0:vw] = (NUM[r0:r0 + rb, :] * COL[r0:r0 + rb, 0:1]).astype(BF16)

    for c in w_copies[7:]:
        c.wait()
    cw = D // RS_CHUNKS

    def out_block(chip_row, idx, j):
        cols = pl.ds(pl.multiple_of(j * cw, 128), cw)
        rr = rows_of(chip_row, 2)
        PS[rr, cols] = mm(HC[rr, :], WO[:, cols]).astype(BF16)
        return remote(PS.at[rows_of(chip_row + 1 - core), cols], DR.at[idx, :, cols],
                      rd_s.at[idx, j], rd_r.at[idx, j], to_tp=partner)

    def pair_sum(chip_row, idx, j):
        cols = pl.ds(pl.multiple_of(j * cw, 128), cw)
        mine_rows = rows_of(chip_row + core)
        remote(PS.at[mine_rows, cols], DR.at[idx, :, cols], rd_s.at[idx, j], rd_r.at[idx, j],
               to_tp=partner).wait_recv()
        return cols, PS[mine_rows, cols].astype(F32) + DR[idx, :, cols].astype(F32)

    def y_copy(k, j):
        cols = pl.ds(pl.multiple_of(j * cw, 128), cw)
        return remote(YS.at[k - 1, :, cols], YR.at[k - 1, :, cols], ry_s.at[k - 1, j], ry_r.at[k - 1, j],
                      to_tp=lax.rem(y + k, n_y) * 2 + core)

    for k in range(1, n_y):
        def one(j, _, k=k):
            @pl.when(j < RS_CHUNKS)
            def _():
                out_block(others[k - 1], k, j).start()

            @pl.when(j > 0)
            def _():
                cols, s = pair_sum(others[k - 1], k, j - 1)
                YS[k - 1, :, cols] = s.astype(BF16)
                y_copy(k, j - 1).start()
            return 0

        lax.fori_loop(0, RS_CHUNKS + 1, one, 0)

    def local(j, _):
        out_block(2 * y, 0, j).start()
        return 0

    lax.fori_loop(0, RS_CHUNKS, local, 0)

    def finish(j, _):
        cols, s = pair_sum(2 * y, 0, j)
        for k in range(1, n_y):
            y_copy(k, j).wait_recv()
            s = s + YR[k - 1, :, cols].astype(F32)
        out[:, cols] = s.astype(BF16)
        return 0

    lax.fori_loop(0, RS_CHUNKS, finish, 0)

    for cp in sends:
        cp.wait_send()
    own.wait_send()

    def drain(j, _):
        for idx in range(n_y):
            cols = pl.ds(pl.multiple_of(j * cw, 128), cw)
            remote(PS.at[rows_of(2 * y + core), cols], DR.at[idx, :, cols], rd_s.at[idx, j],
                   rd_r.at[idx, j], to_tp=partner).wait_send()
        for k in range(1, n_y):
            y_copy(k, j).wait_send()
        return 0

    lax.fori_loop(0, RS_CHUNKS, drain, 0)


def per_device(
    n_sp, n_tp,
    tokens, in_gain, w_query, w_key, w_value, w_input_gate, w_forget_gate, forget_bias,
    forget_extra, w_conv_gate, w_conv_left, w_conv_right, conv_taps, first_memory, first_norm,
    w_out_memory, w_out_conv,
):
    heads = w_query.shape[1] // KEY_DIM
    channels = w_conv_gate.shape[1]
    R, D = tokens.shape
    T = R * n_tp
    n_y = n_tp // 2
    qk, vw = heads * KEY_DIM, heads * VALUE_DIM
    total = 2 * qk + vw + 128 + 3 * channels
    n_heads = w_input_gate.shape[1]
    gates = jnp.concatenate(
        [w_input_gate, w_forget_gate, jnp.zeros((D, 128 - 2 * n_heads), BF16)], axis=1)
    n_st = len(scan_steps(n_sp))
    vmem = pl.BlockSpec(memory_space=pltpu.VMEM)
    hbm = pl.BlockSpec(memory_space=pl.ANY)
    V, dma = pltpu.VMEM, pltpu.SemaphoreType.DMA
    ny1 = n_y - 1
    return pl.pallas_call(
        functools.partial(kernel, n_sp, n_tp, heads, channels, n_heads * VALUE_DIM),
        out_shape=jax.ShapeDtypeStruct((R, D), BF16),
        in_specs=[vmem, vmem] + [hbm] * 7
        + [pl.BlockSpec(memory_space=pltpu.SMEM)] + [vmem] * 4 + [hbm] * 2,
        out_specs=vmem,
        scratch_shapes=[
            V((D, total), BF16), V((vw + channels, D), BF16), V((T, D), BF16), V((T, total), BF16),
            V((T, 128), F32), V((T, 128), F32), V((T, vw), F32), V((heads, T, 128), F32),
            V((T, vw + channels), BF16), V((8 + T, channels), F32),
            V((16, channels), BF16), V((16, channels), BF16),
            V((heads, KEY_DIM, VALUE_DIM), F32), V((heads, KEY_DIM, VALUE_DIM), F32),
            V((n_st, 8, 128), F32), V((n_st, 8, 128), F32),
            V((n_st, heads, KEY_DIM, VALUE_DIM), BF16), V((n_st, heads, KEY_DIM, VALUE_DIM), BF16),
            V((8, T), F32), V((n_tp - 1, 8, T), F32),
            V((T, D), BF16), V((n_y, R, D), BF16), V((ny1, R, D), BF16), V((ny1, R, D), BF16),
            dma((9,)), dma((2,)), dma((ny1, AG_CHUNKS)), dma((ny1, AG_CHUNKS)),
            dma((ny1, AG_CHUNKS)), dma((ny1, AG_CHUNKS)), dma((n_st, 2)), dma((n_st, 2)), dma((2,)),
            dma((n_tp - 1,)), dma((n_tp - 1,)),
            dma((n_y, RS_CHUNKS)), dma((n_y, RS_CHUNKS)), dma((ny1, RS_CHUNKS)), dma((ny1, RS_CHUNKS)),
        ],
        compiler_params=pltpu.CompilerParams(
            collective_id=0, has_side_effects=True, vmem_limit_bytes=60 * 1024 * 1024),
        name="layer",
    )(
        tokens, in_gain.reshape(1, D), w_key, w_value, gates, w_query, w_conv_gate, w_conv_left,
        w_conv_right, forget_bias, forget_extra.T, conv_taps, first_memory, first_norm,
        w_out_memory, w_out_conv,
    )


def solution(mesh):
    in_specs = (
        P(("sp", "tp"), None), P(), P(None, "tp"), P(None, "tp"), P(None, "tp"), P(), P(), P(),
        P("sp", "tp"), P(None, "tp"), P(None, "tp"), P(None, "tp"), P(), P("tp", None, None),
        P("tp", None), P("tp", None), P("tp", None),
    )
    return jax.shard_map(
        functools.partial(per_device, mesh.shape["sp"], mesh.shape["tp"]),
        mesh=mesh, in_specs=in_specs, out_specs=P(("sp", "tp"), None), check_vma=False,
    )
```

time: 205 us -> 84 us (0.41)
  Pallas kernels: 0 us -> 78.3 us
  waiting for transfers between devices: 75.8 us -> 0 us
  blocking collectives: 60.6 us -> 0 us
  matrix products: 37.1 us -> 0 us
  between operations: 14.1 us -> 0.02 us
  other arithmetic: 9.26 us -> 1.12 us
  starting transfers between devices: 4.02 us -> 0 us
    pallas_call x0 -> x1, Pallas kernels: none -> 78.3 us  [per_device(): pl.pallas_call(functools.partial(kernel, n_sp, n_tp, heads, channels, n_h...]
    reduce_scatter x1 -> x0, waiting for transfers between devices: 44.5 us -> none  [per_device(): lax.psum_scatter((jnp.dot(heads_out, w_out_memory, preferred_element_type...]
    dot_general x15 -> x0, matrix products: 37.1 us -> none  [the longest x8 21.1 us: per_device(): jnp.dot(sub_rows, weight, preferred_element_type=jnp.float32)]
    all_gather x2 -> x0, blocking collectives: 37 us -> none  [entering(): gathered = jax.tree.map(lambda a: lax.all_gather(a, axis), part)]
    all_gather x2 -> x0, waiting for transfers between devices: 31.2 us -> none  [the longest x1 31.2 us: per_device(): sub_rows = lax.all_gather(normed, 'tp', axis=0, tiled=True)]
    unnamed x1 -> x0, blocking collectives: 17.7 us -> none
    psum x1 -> x0, blocking collectives: 5.88 us -> none  [per_device(): row_total = lax.psum(local_squares, 'tp')]
    convert_element_type x4 -> x0, other arithmetic: 5.42 us -> none  [the longest x1 2.26 us: per_device(): normed = (token_rows * scale_rows * in_gain).astype(jnp.bfloat16)]
  transfers between devices with their start and end apart: 4 -> 0, of which waited for: 2 -> 0; matrix products, arithmetic and copies ran while one was open for 8% -> 0% of each run, Pallas kernels for 0% -> 0%
where the time goes in v1:
time: 84 us; the launch traced here: 83.7 us
  Pallas kernels  78.3 us (93%)
  local copies, waits for them, and re-layouts  4.23 us (5%)
  other arithmetic  1.12 us (1%)
    pallas_call x1, Pallas kernels, per_device(): pl.pallas_call(functools.partial(kernel, n_sp, n_tp, heads, channels, n_h...  78.3 us
    unnamed x3, local copies, waits for them, and re-layouts  4.15 us

profile of v1, /device:TPU:0, one launch (start us, length us, event | category | flops | bytes accessed | tf_op | source)
XLA Modules:
  0.0 83.7 jit_solution(7058669048066893248)
XLA Ops:
  0.0 0.1 pad.2.clone
  0.1 1.0 %copy.18 = bf16[2048,8]{1,0:T(8,128)(2,1)S(1)} copy(bf16[2048,8]{0,1:T(8,128)(2,1)} %param.22) | data formatting | bytes 65536 | tf_op args[5]
  1.1 1.0 %copy.19 = bf16[2048,8]{1,0:T(8,128)(2,1)S(1)} copy(bf16[2048,8]{0,1:T(8,128)(2,1)} %param.23) | data formatting | bytes 65536 | tf_op args[6]
  2.2 1.1 %maximum_maximum_fusion.wg = bf16[2048,128]{1,0:T(8,128)(2,1)} fusion(bf16[2048,8]{1,0:T(8,128)(2,1)S(1)} %copy.19, bf16[2048,8]{1,0:T(8,128)(2,1)S(1)} %copy.18, bf16[128]{0:T(256)(128)(2,1)S(1)} %pad.2.clone), kind=kLoop, calls=%fused_computation | loop fusion | flops 1572864 | bytes 590080 | tf_op jit(solution)/shard_map/concatenate | solution.py:427
  3.3 78.3 %layer.1 = bf16[192,2048]{1,0:T(8,128)(2,1)} custom-call(bf16[192,2048]{1,0:T(8,128)(2,1)} %tokens.1, f32[1,2048]{1,0:T(1,128)} %bitcast.2, bf16[2048,256]{1,0:T(8,128)(2,1)} %wk.1, bf16[2048,512]{1,0:T(8,128)(2,1)} %wv.1, bf16[2048,128]{1,0:T(8,128)(2,1)} %maximum_maximum_fusion.wg, bf16[2048,256]{1,0:T(8,128)(2,1)} %wq.1, bf16[2048,512]{1,0:T(8,128)(2,1)} %wcg.1, ...), custom_call_target="tpu_custom_call" | custom-call | tf_op jit(solution)/shard_map/layer/pallas_call | solution.py:434
  81.6 2.1 %copy.21 = bf16[192,2048]{1,0:T(8,128)(2,1)} copy(bf16[192,2048]{1,0:T(8,128)(2,1)} %layer.1) | data formatting | bytes 1572864
  (1 shorter events, 0.0 us)

commit v2 on v1

--- a/solution.py
+++ b/solution.py
@@ -37,7 +37,7 @@
 
 def kernel(
     n_sp, n_tp, heads, channels, width,
-    tokens, gain, wk, wv, wg, wq, wcg, wcl, wcr, bias, extra, taps, first_mem, first_norm,
+    tokens, gain, wk, wv, wq, wcg, wcl, wcr, wig, wfg, bias, extra, taps, first_mem, first_norm,
     wom, woc, out,
     W, WO, XG, PJ, G, COL, NUM, DEN, HC, PROD, halo_out, halo_in,
     A_mem, E_mem, sm_out, sm_in, mem_out_b, mem_in_b, sq_out, sq_in,
@@ -60,14 +60,14 @@
     total = o_c + 3 * channels
     steps = scan_steps(n_sp)
 
-    srcs = [(wk, 0, qk), (wv, o_v, vw), (wg, o_g, 128), (wq, o_q, qk), (wcg, o_c, channels),
+    srcs = [(wk, 0, qk), (wv, o_v, vw), (wq, o_q, qk), (wcg, o_c, channels),
             (wcl, o_c + channels, channels), (wcr, o_c + 2 * channels, channels)]
     w_copies = [
         pltpu.make_async_copy(s, W.at[:, pl.ds(o, n)], w_sem.at[i])
         for i, (s, o, n) in enumerate(srcs)
     ]
-    w_copies.append(pltpu.make_async_copy(wom, WO.at[pl.ds(0, vw), :], w_sem.at[7]))
-    w_copies.append(pltpu.make_async_copy(woc, WO.at[pl.ds(vw, channels), :], w_sem.at[8]))
+    w_copies.append(pltpu.make_async_copy(wom, WO.at[pl.ds(0, vw), :], w_sem.at[6]))
+    w_copies.append(pltpu.make_async_copy(woc, WO.at[pl.ds(vw, channels), :], w_sem.at[7]))
     for c in w_copies:
         c.start()
 
@@ -122,12 +122,16 @@
         rr = rows_of(block, 2)
         G[rr, :] = mm(XG[rr, :], W[:, o_g:o_g + 128])
 
+    n_heads = bias.shape[0]
+    W[:, o_g:o_g + 128] = jnp.concatenate(
+        [wig[...].astype(F32), wfg[...].astype(F32), jnp.zeros((128 - 2 * n_heads, D), F32)],
+        axis=0).T.astype(BF16)
     own.wait_recv()
-    for c in w_copies[:3]:
+    for c in w_copies[:2]:
         c.wait()
     project(2 * y, 0, o_g)
     project_gates(2 * y)
-    for c in w_copies[3:7]:
+    for c in w_copies[2:6]:
         c.wait()
     project(2 * y, o_q, total)
     fwd = []
@@ -149,7 +153,6 @@
         project(b, 0, o_g)
         project_gates(b)
 
-    n_heads = bias.shape[0]
     gt = G[...].T
     in_all, forget_all = gt[0:n_heads], gt[n_heads:2 * n_heads]
     sub = lax.broadcasted_iota(jnp.int32, (n_heads, T), 0)
@@ -168,95 +171,85 @@
     for d in scan_steps(T):
         cum = cum + jnp.where(lane >= d, pltpu.roll(cum, d, 1), 0.0)
     gap = in_pre - cum
-    run = gap
-    for d in scan_steps(T):
-        run = jnp.maximum(run, jnp.where(lane >= d, pltpu.roll(run, d, 1), run))
     decay = cum[:, T - 1:T]
-    gmax = run[:, T - 1:T]
-    COL[...] = jnp.concatenate(
-        [gap, run, jnp.exp(gap - gmax), jnp.zeros((104, T), F32)], axis=0).T
+    gmax = jnp.max(gap, axis=1, keepdims=True)
+    COL[...] = jnp.concatenate([jnp.exp(gap - gmax), jnp.zeros((120, T), F32)], axis=0).T
     ones = jnp.ones((1, 128), F32)
-
-    sm = jnp.zeros((8, 128), F32)
     s8 = lax.broadcasted_iota(jnp.int32, (8, 128), 0)
+
+    def state_copies(i, h):
+        to = lax.rem(sp + steps[i], n_sp)
+        return (remote(mem_out_b.at[i, h], mem_in_b.at[i, h], st_s.at[i, h, 0], st_r.at[i, h, 0], to_sp=to),
+                remote(sm_out.at[i, h], sm_in.at[i, h], st_s.at[i, h, 1], st_r.at[i, h, 1], to_sp=to))
+
+    def state_send(i, h, vec, mem):
+        n, d, m = vec
+        mem_out_b[i, h] = mem.astype(BF16)
+        sm_out[i, h] = jnp.where(s8 == 0, n, jnp.where(s8 == 1, d, m))
+        for cp in state_copies(i, h):
+            cp.start()
+            sends.append(cp)
+
+    zero = jnp.zeros((1, 128), F32)
+    incl, excl = [None] * heads, [(zero, zero, jnp.full((1, 128), NEG, F32))] * heads
     for h in range(heads):
-        keyed = PJ[:, h * KEY_DIM:(h + 1) * KEY_DIM].astype(F32) * COL[:, 16 + h:17 + h]
+        keyed = PJ[:, h * KEY_DIM:(h + 1) * KEY_DIM].astype(F32) * COL[:, h:h + 1]
         norm = jnp.sum(keyed, axis=0, keepdims=True)
         mem = mm(keyed.T.astype(BF16), PJ[:, o_v + h * VALUE_DIM:o_v + (h + 1) * VALUE_DIM])
         A_mem[h] = mem
-        mem_out_b[0, h] = mem.astype(BF16)
-        sm = jnp.where(s8 == h, norm, sm)
-        sm = jnp.where(s8 == heads + h, decay[h:h + 1] * ones, sm)
-        sm = jnp.where(s8 == 2 * heads + h, (decay[h:h + 1] + gmax[h:h + 1]) * ones, sm)
+        incl[h] = (norm, decay[h:h + 1] * ones, (decay[h:h + 1] + gmax[h:h + 1]) * ones)
+        state_send(0, h, incl[h], mem)
     E_mem[...] = jnp.zeros_like(E_mem)
-    sm_out[0] = sm
-
-    def state_copies(i, forward):
-        d = steps[i]
-        to = lax.rem(sp + d, n_sp)
-        return (remote(mem_out_b.at[i], mem_in_b.at[i], st_s.at[i, 0], st_r.at[i, 0], to_sp=to),
-                remote(sm_out.at[i], sm_in.at[i], st_s.at[i, 1], st_r.at[i, 1], to_sp=to))
-
-    def state_send(i):
-        for cp in state_copies(i, True):
-            cp.start()
-            sends.append(cp)
-
-    def part(s, j, h):
-        return s[j * heads + h:j * heads + h + 1]
-
-    def join(valid, early, early_mem, late, late_mem, h):
-        n_e, d_e, m_e = part(early, 0, h), part(early, 1, h), part(early, 2, h)
-        n_l, d_l, m_l = part(late, 0, h), part(late, 1, h), part(late, 2, h)
+
+    def join(valid, early, early_mem, late, late_mem):
+        n_e, d_e, m_e = early
+        n_l, d_l, m_l = late
         d_e = jnp.where(valid, d_e, 0.0)
         m_e = jnp.where(valid, m_e, NEG)
         top = jnp.maximum(m_e + d_l, m_l)
         s_e = jnp.where(valid, jnp.exp(m_e + d_l - top), 0.0)
         s_l = jnp.exp(m_l - top)
-        return (s_e * n_e + s_l * n_l, d_e + d_l, top,
+        return ((s_e * n_e + s_l * n_l, d_e + d_l, top),
                 s_e[:, 0:1] * early_mem + s_l[:, 0:1] * late_mem)
 
-    state = {"a": sm, "e": jnp.where(s8 >= 2 * heads, NEG, 0.0)}
-
-    def state_step(i):
-        for cp in state_copies(i, False):
+    def state_step(i, h):
+        for cp in state_copies(i, h):
             cp.wait_recv()
         valid = sp >= steps[i]
-        got = sm_in[i]
-        last = i + 1 == len(steps)
-        for which, ref in (("e", E_mem), ("a", A_mem)):
-            if which == "a" and last:
-                continue
-            new = jnp.zeros((8, 128), F32)
-            for h in range(heads):
-                n_j, d_j, m_j, mem = join(valid, got, mem_in_b[i, h].astype(F32), state[which], ref[h], h)
-                ref[h] = mem
-                if which == "a":
-                    mem_out_b[i + 1, h] = mem.astype(BF16)
-                new = jnp.where(s8 == h, n_j, new)
-                new = jnp.where(s8 == heads + h, d_j, new)
-                new = jnp.where(s8 == 2 * heads + h, m_j, new)
-            state[which] = new
-            if which == "a":
-                sm_out[i + 1] = new
-        if not last:
-            state_send(i + 1)
-
-    state_send(0)
-    for b in others:
-        project(b, o_q, total)
+        got = sm_in[i, h]
+        early = (got[0:1], got[1:2], got[2:3])
+        early_mem = mem_in_b[i, h].astype(F32)
+        if i + 1 < len(steps):
+            incl[h], mem = join(valid, early, early_mem, incl[h], A_mem[h])
+            A_mem[h] = mem
+            state_send(i + 1, h, incl[h], mem)
+        excl[h], mem = join(valid, early, early_mem, excl[h], E_mem[h])
+        E_mem[h] = mem
+
+    def work_running_max():
+        run = gap
+        for d in scan_steps(T):
+            run = jnp.maximum(run, jnp.where(lane >= d, pltpu.roll(run, d, 1), run))
+        COL[...] = jnp.concatenate([run, jnp.zeros((120, T), F32)], axis=0).T
 
     rb = 256 if T % 256 == 0 else R
-    for r0 in range(0, T, rb):
-        left = PJ[r0:r0 + rb, o_c + channels:o_c + 2 * channels].astype(F32)
-        right = PJ[r0:r0 + rb, o_c + 2 * channels:o_c + 3 * channels].astype(F32)
-        prod = (left * right).astype(BF16)
-        PROD[8 + r0:8 + r0 + rb, :] = prod.astype(F32)
-        if r0 + rb == T:
-            halo_out[...] = prod[rb - 16:rb]
+
+    def work_project(first, last):
+        for b in others:
+            project(b, first, last)
+
     halo = remote(halo_out, halo_in, hl_s.at[0], hl_s.at[1], to_sp=lax.rem(sp + 1, n_sp))
-    halo.start()
-    sends.append(halo)
+
+    def work_product():
+        for r0 in range(0, T, rb):
+            left = PJ[r0:r0 + rb, o_c + channels:o_c + 2 * channels].astype(F32)
+            right = PJ[r0:r0 + rb, o_c + 2 * channels:o_c + 3 * channels].astype(F32)
+            prod = (left * right).astype(BF16)
+            PROD[8 + r0:8 + r0 + rb, :] = prod.astype(F32)
+            if r0 + rb == T:
+                halo_out[...] = prod[rb - 16:rb]
+        halo.start()
+        sends.append(halo)
 
     q_scale = KEY_DIM ** -0.5
 
@@ -268,7 +261,7 @@
         s = mm_t(q, k) * q_scale
         ti = lax.broadcasted_iota(jnp.int32, (rb, e), 0) + r0
         si = lax.broadcasted_iota(jnp.int32, (rb, e), 1)
-        w = jnp.where(ti >= si, gap[h:h + 1, 0:e] - COL[r0:e, 8 + h:9 + h], NEG)
+        w = jnp.where(ti >= si, gap[h:h + 1, 0:e] - COL[r0:e, h:h + 1], NEG)
         mix = s * jnp.exp(w)
         DEN[h, r0:e, :] = jnp.broadcast_to(jnp.sum(mix, axis=1, keepdims=True), (rb, 128))
         NUM[r0:e, h * VALUE_DIM:(h + 1) * VALUE_DIM] = mm(mix.astype(BF16), v)
@@ -287,22 +280,28 @@
             gate = PJ[r0:r0 + rb, o_c:o_c + channels].astype(F32)
             HC[r0:r0 + rb, vw:] = (gate * f).astype(BF16)
 
-    work.append(conv_finish)
-    share = -(-len(work) // len(steps))
-    for i in range(len(steps)):
-        state_step(i)
-        if i + 1 < len(steps):
-            for w_ in work[:share]:
-                w_()
-            work = work[share:]
-        elif work:
-            for w_ in work:
-                w_()
-
-    e_s = state["e"]
+    c1 = o_c + channels
+    slots = [
+        [functools.partial(work_project, o_q, c1), work_running_max],
+        [functools.partial(work_project, c1, total)],
+        [work_product, work.pop(0)],
+    ]
+    events = [(i, h) for i in range(len(steps)) for h in range(heads)]
+    rest = work + [conv_finish]
+    for n, event in enumerate(events[:-heads]):
+        for w_ in (slots.pop(0) if slots else [rest.pop(0)] if rest else []):
+            w_()
+        state_step(*event)
+    for group in slots:
+        for w_ in group:
+            w_()
+    for w_ in rest:
+        w_()
+
     sq = [jnp.zeros((rb, 1), F32) for _ in range(T // rb)]
     for h in range(heads):
-        n_e, d_e, m_e = part(e_s, 0, h), part(e_s, 1, h), part(e_s, 2, h)
+        state_step(len(steps) - 1, h)
+        n_e, d_e, m_e = excl[h]
         cmax = jnp.maximum(m_e, d_e)
         s_p, s_f = jnp.exp(m_e - cmax), jnp.exp(d_e - cmax)
         c_mem = s_p[:, 0:1] * E_mem[h] + s_f[:, 0:1] * first_mem[h]
@@ -314,7 +313,7 @@
             q = PJ[r0:e, o_q + h * KEY_DIM:o_q + (h + 1) * KEY_DIM]
             fm = mm(q, hi) + mm(q, lo)
             fn = jnp.sum(q.astype(F32) * c_norm, axis=1, keepdims=True)
-            m0 = COL[r0:e, 8 + h:9 + h]
+            m0 = COL[r0:e, h:h + 1]
             m = jnp.maximum(m0, cmax[:, 0:1])
             k0 = jnp.exp(m0 - m)
             k1 = jnp.exp(cmax[:, 0:1] - m) * q_scale
@@ -340,7 +339,7 @@
     for r0 in range(0, T, rb):
         HC[r0:r0 + rb, 0:vw] = (NUM[r0:r0 + rb, :] * COL[r0:r0 + rb, 0:1]).astype(BF16)
 
-    for c in w_copies[7:]:
+    for c in w_copies[6:]:
         c.wait()
     cw = D // RS_CHUNKS
 
@@ -424,8 +423,6 @@
     qk, vw = heads * KEY_DIM, heads * VALUE_DIM
     total = 2 * qk + vw + 128 + 3 * channels
     n_heads = w_input_gate.shape[1]
-    gates = jnp.concatenate(
-        [w_input_gate, w_forget_gate, jnp.zeros((D, 128 - 2 * n_heads), BF16)], axis=1)
     n_st = len(scan_steps(n_sp))
     vmem = pl.BlockSpec(memory_space=pltpu.VMEM)
     hbm = pl.BlockSpec(memory_space=pl.ANY)
@@ -434,7 +431,7 @@
     return pl.pallas_call(
         functools.partial(kernel, n_sp, n_tp, heads, channels, n_heads * VALUE_DIM),
         out_shape=jax.ShapeDtypeStruct((R, D), BF16),
-        in_specs=[vmem, vmem] + [hbm] * 7
+        in_specs=[vmem, vmem] + [hbm] * 6 + [vmem] * 2
         + [pl.BlockSpec(memory_space=pltpu.SMEM)] + [vmem] * 4 + [hbm] * 2,
         out_specs=vmem,
         scratch_shapes=[
@@ -443,12 +440,12 @@
             V((T, vw + channels), BF16), V((8 + T, channels), F32),
             V((16, channels), BF16), V((16, channels), BF16),
             V((heads, KEY_DIM, VALUE_DIM), F32), V((heads, KEY_DIM, VALUE_DIM), F32),
-            V((n_st, 8, 128), F32), V((n_st, 8, 128), F32),
+            V((n_st, heads, 8, 128), F32), V((n_st, heads, 8, 128), F32),
             V((n_st, heads, KEY_DIM, VALUE_DIM), BF16), V((n_st, heads, KEY_DIM, VALUE_DIM), BF16),
             V((8, T), F32), V((n_tp - 1, 8, T), F32),
             V((T, D), BF16), V((n_y, R, D), BF16), V((ny1, R, D), BF16), V((ny1, R, D), BF16),
-            dma((9,)), dma((2,)), dma((ny1, AG_CHUNKS)), dma((ny1, AG_CHUNKS)),
-            dma((ny1, AG_CHUNKS)), dma((ny1, AG_CHUNKS)), dma((n_st, 2)), dma((n_st, 2)), dma((2,)),
+            dma((8,)), dma((2,)), dma((ny1, AG_CHUNKS)), dma((ny1, AG_CHUNKS)),
+            dma((ny1, AG_CHUNKS)), dma((ny1, AG_CHUNKS)), dma((n_st, heads, 2)), dma((n_st, heads, 2)), dma((2,)),
             dma((n_tp - 1,)), dma((n_tp - 1,)),
             dma((n_y, RS_CHUNKS)), dma((n_y, RS_CHUNKS)), dma((ny1, RS_CHUNKS)), dma((ny1, RS_CHUNKS)),
         ],
@@ -456,8 +453,8 @@
             collective_id=0, has_side_effects=True, vmem_limit_bytes=60 * 1024 * 1024),
         name="layer",
     )(
-        tokens, in_gain.reshape(1, D), w_key, w_value, gates, w_query, w_conv_gate, w_conv_left,
-        w_conv_right, forget_bias, forget_extra.T, conv_taps, first_memory, first_norm,
+        tokens, in_gain.reshape(1, D), w_key, w_value, w_query, w_conv_gate, w_conv_left,
+        w_conv_right, w_input_gate.T, w_forget_gate.T, forget_bias, forget_extra.T, conv_taps, first_memory, first_norm,
         w_out_memory, w_out_conv,
     )
 

time: 84 us -> 75.2 us (0.90)
  Pallas kernels: 78.3 us -> 72.9 us
  local copies, waits for them, and re-layouts: 4.23 us -> 2.09 us
  other arithmetic: 1.12 us -> 0 us
    pallas_call x1, Pallas kernels: 78.3 us -> 72.9 us  [per_device(): pl.pallas_call(functools.partial(kernel, n_sp, n_tp, heads, channels, n_h...]
    unnamed x3 -> x1, local copies, waits for them, and re-layouts: 4.15 us -> 2.09 us
    concatenate x1 -> x0, other arithmetic: 1.12 us -> none  [per_device(): jnp.concatenate([w_input_gate, w_forget_gate, jnp.zeros((D, 128 - 2 * n_h...]
where the time goes in v2:
time: 75.2 us; the launch traced here: 75 us
  Pallas kernels  72.9 us (97%)
  local copies, waits for them, and re-layouts  2.09 us (3%)
    pallas_call x1, Pallas kernels, per_device(): pl.pallas_call(functools.partial(kernel, n_sp, n_tp, heads, channels, n_h...  72.9 us
    unnamed x1, local copies, waits for them, and re-layouts  2.09 us

profile of v2, /device:TPU:0, one launch (start us, length us, event | category | flops | bytes accessed | tf_op | source)
XLA Modules:
  0.0 75.0 jit_solution(9888528855857844532)
XLA Ops:
  0.0 72.9 %layer.1 = bf16[192,2048]{1,0:T(8,128)(2,1)} custom-call(bf16[192,2048]{1,0:T(8,128)(2,1)} %tokens.1, f32[1,2048]{1,0:T(1,128)} %bitcast.6, bf16[2048,256]{1,0:T(8,128)(2,1)} %wk.1, bf16[2048,512]{1,0:T(8,128)(2,1)} %wv.1, bf16[2048,256]{1,0:T(8,128)(2,1)} %wq.1, bf16[2048,512]{1,0:T(8,128)(2,1)} %wcg.1, bf16[2048,512]{1,0:T(8,128)(2,1)} %wcl.1, ...), custom_call_target="tpu_custom_call" | custom-call | tf_op jit(solution)/shard_map/layer/pallas_call | solution.py:431
  72.9 2.1 %copy.19 = bf16[192,2048]{1,0:T(8,128)(2,1)} copy(bf16[192,2048]{1,0:T(8,128)(2,1)} %layer.1) | data formatting | bytes 1572864
